TPU v7x, 32 devices: a whole 2x2x4 slice. The times are simulated.
32 devices in a mesh: ep: 16 (over z, y, x), tp: 2 (over core).
Axes of the slice: x: 2, y: 2, z: 4, core: 2. Of those that a mesh axis runs over, the one named last changes fastest.
Arguments:
- tokens: bfloat16 [64, 4096], P('ep'), may hold values from -6 to 6
- memory: float32 [64, 8, 256, 512], P('ep', 'tp'), may hold values from -6 to 6
- normalizer: float32 [64, 8, 256], P('ep', 'tp'), may hold values from -6 to 6
- stabilizer: float32 [64, 8], P('ep', 'tp'), may hold values from -4 to 4
- norm_gain: float32 [4096], replicated, may hold values from 0.1 to 1.9
- w_query: bfloat16 [4096, 8, 256], P(None, 'tp', 'ep'), may hold values from -0.09375 to 0.09375
- w_key: bfloat16 [4096, 8, 256], P(None, 'tp', 'ep'), may hold values from -0.09375 to 0.09375
- w_value: bfloat16 [4096, 8, 512], P(None, 'tp', 'ep'), may hold values from -0.09375 to 0.09375
- w_outgate: bfloat16 [4096, 8, 512], P(None, 'tp', 'ep'), may hold values from -0.09375 to 0.09375
- w_input: bfloat16 [4096, 8], P(None, 'tp'), may hold values from -0.09375 to 0.09375
- w_forget: bfloat16 [4096, 8], P(None, 'tp'), may hold values from -0.09375 to 0.09375
- forget_bias: float32 [8], P('tp'), may hold values from 0 to 4
- w_out: bfloat16 [4096, 4096], P('tp', 'ep'), may hold values from -0.09375 to 0.09375
- ffn_gain: float32 [4096], replicated, may hold values from 0.1 to 1.9
- w_gate: bfloat16 [16, 4096, 512], P('ep', None, 'tp'), may hold values from -0.09375 to 0.09375
- w_up: bfloat16 [16, 4096, 512], P('ep', None, 'tp'), may hold values from -0.09375 to 0.09375
- w_down: bfloat16 [16, 512, 4096], P('ep', 'tp'), may hold values from -0.25 to 0.25
- expert_ids: int32 [64, 2], P('ep'), may hold values from 0 to 15, as said below
- route_weights: float32 [64, 2], P('ep'), may hold values from 0.1 to 1
Outputs:
- out: bfloat16 [64, 4096], P('ep')
- memory_next: float32 [64, 8, 256, 512], P('ep', 'tp')
- normalizer_next: float32 [64, 8, 256], P('ep', 'tp')
- stabilizer_next: float32 [64, 8], P('ep', 'tp')
Inputs may be any that keep to these rules, and one draw needn't show every extreme that they name: `expert_ids`: the 2 experts of a token differ and lie in one group of 8 consecutive experts. Beyond that, any choice is allowed: for instance, all 4 tokens of one index of ep may name the same expert.
All inputs are finite; a program needn't handle non-finite values.
Results may differ from a plain program's by a relative error of at most 0.013.
Values may be sent and summed in bfloat16 or wider, within the bound.
No kernel may reach another device: no remote copies, remote signals or barrier semaphores. Data moves between devices by JAX's collectives and lax.ppermute only.
A program may use at most 128 MiB of HBM per device.

v0:
```python
import jax
import jax.numpy as jnp
from jax import lax
from jax.sharding import PartitionSpec as P


def rms_scale(values, gain):
    return values * lax.rsqrt(jnp.mean(values * values, axis=-1, keepdims=True) + 1e-06) * gain


def product(left, right):
    return jnp.dot(left, right, preferred_element_type=jnp.float32)


def rounded_term(values):
    return lax.optimization_barrier(values.astype(jnp.bfloat16)).astype(jnp.float32)


def body(
    tokens,
    memory,
    normalizer,
    stabilizer,
    norm_gain,
    w_query,
    w_key,
    w_value,
    w_outgate,
    w_input,
    w_forget,
    forget_bias,
    w_out,
    ffn_gain,
    w_gate,
    w_up,
    w_down,
    expert_ids,
    route_weights,
):
    seqs, width = tokens.shape
    heads, key_size, value_size = (memory.shape[1], memory.shape[2], memory.shape[3])
    value_width = heads * value_size
    key_piece = w_query.shape[2]
    value_piece = w_value.shape[2]
    query_cols = w_query.reshape(width, heads * key_piece)
    key_cols = w_key.reshape(width, heads * key_piece)
    value_cols = w_value.reshape(width, heads * value_piece)
    outgate_cols = w_outgate.reshape(width, heads * value_piece)
    normed = rms_scale(tokens.astype(jnp.float32), norm_gain).astype(jnp.bfloat16)
    piece = lax.all_gather(normed, "ep", axis=0, tiled=True)
    projected = jnp.concatenate(
        [
            product(piece, query_cols),
            product(piece, key_cols),
            product(piece, value_cols),
            product(piece, outgate_cols),
        ],
        axis=1,
    ).astype(jnp.bfloat16)
    all_rows = projected.shape[0]
    narrow = heads * key_piece
    broad = heads * value_piece
    query_part = projected[:, :narrow].reshape(all_rows, heads, key_piece)
    key_part = projected[:, narrow : 2 * narrow].reshape(all_rows, heads, key_piece)
    value_part = projected[:, 2 * narrow : 2 * narrow + broad].reshape(all_rows, heads, value_piece)
    outgate_part = projected[:, 2 * narrow + broad :].reshape(all_rows, heads, value_piece)
    query, key, value, outgate = (
        lax.all_to_all(query_part, "ep", split_axis=0, concat_axis=2, tiled=True),
        lax.all_to_all(key_part, "ep", split_axis=0, concat_axis=2, tiled=True),
        lax.all_to_all(value_part, "ep", split_axis=0, concat_axis=2, tiled=True),
        lax.all_to_all(outgate_part, "ep", split_axis=0, concat_axis=2, tiled=True),
    )
    in_pre = product(normed, w_input)
    log_forget = jax.nn.log_sigmoid(product(normed, w_forget) + forget_bias)
    scaled = query.astype(jnp.float32) * key_size ** (-0.5)
    key_heads = key.astype(jnp.float32)
    value_heads = value.astype(jnp.float32)
    stab_next = jnp.maximum(log_forget + stabilizer, in_pre)
    decay = jnp.exp(log_forget + stabilizer - stab_next)
    inweight = jnp.exp(in_pre - stab_next)
    memory_next = decay[:, :, None, None] * memory + inweight[:, :, None, None] * (
        key_heads[:, :, :, None] * value_heads[:, :, None, :]
    )
    normalizer_next = decay[:, :, None] * normalizer + inweight[:, :, None] * key_heads
    numerator = jnp.einsum("shd,shde->she", scaled, memory_next, precision=lax.Precision.HIGHEST)
    denominator = jnp.sum(scaled * normalizer_next, axis=-1)
    hidden = numerator / jnp.maximum(jnp.abs(denominator), jnp.exp(-stab_next))[:, :, None]
    hidden = (
        hidden.reshape(seqs, value_width)
        * jax.nn.sigmoid(outgate.reshape(seqs, value_width).astype(jnp.float32))
    ).astype(jnp.bfloat16)
    partial_value = product(lax.all_gather(hidden, "ep", axis=0, tiled=True), w_out)
    summed = lax.psum(rounded_term(partial_value).astype(jnp.bfloat16), "tp")
    mixed = lax.all_to_all(summed, "ep", split_axis=0, concat_axis=1, tiled=True)
    resid = tokens.astype(jnp.float32) + mixed.astype(jnp.float32)
    ffn_in = rms_scale(resid, ffn_gain).astype(jnp.bfloat16)
    gate_local, up_local, down_local = (w_gate[0], w_up[0], w_down[0])
    n_experts = lax.axis_size("ep") * w_gate.shape[0]
    piece = lax.all_gather(ffn_in, "ep", axis=0, tiled=True)
    gate_part = product(piece, gate_local)
    up_part = product(piece, up_local)
    act = (jax.nn.silu(gate_part) * up_part).astype(jnp.bfloat16)
    expert_terms = rounded_term(product(act, down_local))
    labels = jnp.arange(n_experts, dtype=jnp.int32)
    route_dense = jnp.sum(
        jnp.where(expert_ids[:, :, None] == labels[None, None, :], route_weights[:, :, None], 0.0),
        axis=1,
    )
    my_weight = lax.all_to_all(route_dense, "ep", split_axis=1, concat_axis=0, tiled=True)
    contrib = expert_terms * my_weight
    n_ep = lax.axis_size("ep")
    n_tp = lax.axis_size("tp")
    arranged = jnp.swapaxes(contrib.reshape(n_ep, seqs, n_tp, width // n_tp), 1, 2)
    arranged = arranged.reshape(n_ep * n_tp * seqs, width // n_tp)
    mine = lax.psum_scatter(arranged, ("ep", "tp"), scatter_dimension=0, tiled=True)
    ffn_out = lax.all_gather(mine.astype(jnp.bfloat16), "tp", axis=1, tiled=True).astype(mine.dtype)
    out = (resid + ffn_out).astype(jnp.bfloat16)
    return (out, memory_next, normalizer_next, stab_next)


def solution(mesh):
    return jax.shard_map(
        body,
        mesh=mesh,
        in_specs=(
            P("ep", None),
            P("ep", "tp", None, None),
            P("ep", "tp", None),
            P("ep", "tp"),
            P(),
            P(None, "tp", "ep"),
            P(None, "tp", "ep"),
            P(None, "tp", "ep"),
            P(None, "tp", "ep"),
            P(None, "tp"),
            P(None, "tp"),
            P("tp"),
            P("tp", "ep"),
            P(),
            P("ep", None, "tp"),
            P("ep", None, "tp"),
            P("ep", "tp", None),
            P("ep", None),
            P("ep", None),
        ),
        out_specs=(P("ep", None), P("ep", "tp", None, None), P("ep", "tp", None), P("ep", "tp")),
        check_vma=False,
    )
```

profile of v0, /device:TPU:0, one launch (start us, length us, event | category | flops | bytes accessed | tf_op | source)
XLA Modules:
  0.0 274.0 jit_solution(16929384175384432204)
XLA Ops:
  0.7 1.1 fusion.14
  1.7 0.9 fusion.49
  2.6 45.3 %all-gather = bf16[16,4,4096]{2,1,0:T(4,128)(2,1)S(1)} all-gather(bf16[1,4,4096]{2,1,0:T(4,128)(2,1)S(1)} %fusion.49), channel_id=1, replica_groups=mesh['ep'=16,'tp'=2] {'ep'}, dimensions={0}, use_global_device_ids=true | all-gather | bytes 557056 | tf_op jit(solution)/shard_map/all_gather | solution.py:50
  48.0 1.3 convolution_convert_fusion.4
  49.5 0.1 copy.119
  49.6 0.7 reshape.153
  50.3 3.5 %all-to-all-start.1 = ((bf16[16,2,128]{2,1,0:T(2,128)(2,1)}), bf16[16,2,128]{2,1,0:T(2,128)(2,1)S(1)}, u32[]{:S(2)}, u32[]{:S(2)}) async-start(bf16[16,2,128]{2,1,0:T(2,128)(2,1)} %reshape.153), calls=%async_computation.1 | async-start | bytes 16384 | tf_op jit(solution)/shard_map/all_to_all | solution.py:69
  53.8 0.8 fusion.16
  54.6 0.9 fusion.29
  55.5 0.9 subtract_exponential_fusion.1
  56.5 1.3 convolution_convert_fusion.5
  57.9 1.7 convolution_convert_fusion.3
  59.6 1.7 convolution_convert_fusion.2
  61.3 0.8 select_reduce_fusion
  62.2 0.1 copy.114
  62.3 0.7 reshape.149
  63.1 0.1 copy.123
  63.2 0.7 reshape.151
  64.1 0.1 copy.127
  64.2 0.7 reshape.155
  64.9 0.7 copy.131
  65.6 6.9 %all-to-all-start = ((bf16[16,2,128]{2,1,0:T(2,128)(2,1)}), bf16[16,2,128]{2,1,0:T(2,128)(2,1)S(1)}, u32[]{:S(2)}, u32[]{:S(2)}) async-start(bf16[16,2,128]{2,1,0:T(2,128)(2,1)} %reshape.149), calls=%async_computation | async-start | bytes 16384 | tf_op jit(solution)/shard_map/all_to_all | solution.py:68
  72.7 7.0 %all-to-all-done = bf16[16,2,128]{2,1,0:T(2,128)(2,1)S(1)} async-done(((bf16[16,2,128]{2,1,0:T(2,128)(2,1)}), bf16[16,2,128]{2,1,0:T(2,128)(2,1)S(1)}, u32[]{:S(2)}, u32[]{:S(2)}) %all-to-all-start) | async-done | bytes 8224 | tf_op jit(solution)/shard_map/all_to_all | solution.py:68
  79.7 3.5 %all-to-all-start.2 = ((bf16[16,2,256]{2,1,0:T(2,128)(2,1)}), bf16[16,2,256]{2,1,0:T(2,128)(2,1)S(1)}, u32[]{:S(2)}, u32[]{:S(2)}) async-start(bf16[16,2,256]{2,1,0:T(2,128)(2,1)} %reshape.151), calls=%async_computation.2 | async-start | bytes 32768 | tf_op jit(solution)/shard_map/all_to_all | solution.py:70
  83.6 0.7 multiply_reduce_fusion.1
  84.5 6.1 %all-to-all-done.2 = bf16[16,2,256]{2,1,0:T(2,128)(2,1)S(1)} async-done(((bf16[16,2,256]{2,1,0:T(2,128)(2,1)}), bf16[16,2,256]{2,1,0:T(2,128)(2,1)S(1)}, u32[]{:S(2)}, u32[]{:S(2)}) %all-to-all-start.2) | async-done | bytes 16416 | tf_op jit(solution)/shard_map/all_to_all | solution.py:70
  90.6 3.5 %all-to-all-start.3 = ((bf16[16,2,256]{2,1,0:T(2,128)(2,1)}), bf16[16,2,256]{2,1,0:T(2,128)(2,1)S(1)}, u32[]{:S(2)}, u32[]{:S(2)}) async-start(bf16[16,2,256]{2,1,0:T(2,128)(2,1)} %reshape.155), calls=%async_computation.3 | async-start | bytes 32768 | tf_op jit(solution)/shard_map/all_to_all | solution.py:71
  94.3 4.2 %multiply_add_fusion = f32[4,4,256,512]{3,2,1,0:T(8,128)S(1)} fusion(f32[4,4,256,512]{3,2,1,0:T(8,128)} %param.20, f32[4,4,512]{2,1,0:T(4,128)S(1)} %reshape.121, f32[4,4,256]{2,1,0:T(4,128)S(1)} %reshape.120, f32[4,4]{1,0:T(4,128)S(1)} %subtract_exponential_fusion, f32[4,4]{1,0:T(4,128)S(1)} %get-tuple-element.6), kind=kLoop, calls=%fused_computation | loop fusion | flops 8388608 | bytes 16826496 | tf_op jit(solution)/shard_map/add | solution.py:81
  98.5 3.4 %copy-done.1 = f32[4,4,256,512]{3,2,1,0:T(8,128)} copy-done((f32[4,4,256,512]{3,2,1,0:T(8,128)}, f32[4,4,256,512]{3,2,1,0:T(8,128)S(1)}, u32[]{:S(2)}) %copy-start.1) | copy-done | bytes 8388632
  101.9 4.0 %fusion.30 = f32[4,4,1,512]{3,2,1,0:T(1,128)S(1)} fusion(f32[4,4,256,1]{2,3,1,0:T(1,128)S(1)} %reshape.141, f32[4,4,256,512]{3,2,1,0:T(8,128)S(1)} %multiply_add_fusion), kind=kOutput, calls=%fused_computation.57 | convolution fusion | flops 25165824 | bytes 8437760 | tf_op jit(solution)/shard_map/shd,shde->she/dot_general | solution.py:85
  106.1 6.9 %all-to-all-start.5 = ((f32[4,16,1]{0,2,1:T(1,128)}), f32[4,16,1]{0,2,1:T(1,128)S(1)}, u32[]{:S(2)}, u32[]{:S(2)}) async-start(f32[4,16,1]{0,2,1:T(1,128)} %copy.131), calls=%async_computation.5 | async-start | bytes 16384 | tf_op jit(solution)/shard_map/all_to_all | solution.py:109
  113.5 42.4 %all-gather.1 = bf16[16,4,2048]{2,1,0:T(4,128)(2,1)S(1)} all-gather(bf16[1,4,2048]{2,1,0:T(4,128)(2,1)S(1)} %fusion.25), channel_id=1, replica_groups=mesh['ep'=16,'tp'=2] {'ep'}, dimensions={0}, use_global_device_ids=true | all-gather | bytes 278528 | tf_op jit(solution)/shard_map/all_gather | solution.py:92
  155.8 0.8 reshape.135
  156.6 1.2 convolution_convert_fusion.1
  157.9 4.0 %psum.7 = bf16[16,4,256]{2,1,0:T(4,128)(2,1)} all-reduce(bf16[16,4,256]{2,1,0:T(4,128)(2,1)S(1)} %all_to_all.24), channel_id=1, replica_groups=mesh['ep'=16,'tp'=2] {'tp'}, use_global_device_ids=true, to_apply=%region_2.3 | all-reduce | flops 16384 | bytes 65536 | tf_op jit(solution)/shard_map/psum | solution.py:93
  161.9 3.5 %all-to-all-start.4 = ((bf16[16,4,256]{2,1,0:T(4,128)(2,1)}), bf16[16,4,256]{2,1,0:T(4,128)(2,1)S(1)}, u32[]{:S(2)}, u32[]{:S(2)}) async-start(bf16[16,4,256]{2,1,0:T(4,128)(2,1)} %psum.7), calls=%async_computation.4 | async-start | bytes 65536 | tf_op jit(solution)/shard_map/all_to_all | solution.py:94
  165.5 7.3 %all-to-all-done.4 = bf16[16,4,256]{2,1,0:T(4,128)(2,1)S(1)} async-done(((bf16[16,4,256]{2,1,0:T(4,128)(2,1)}), bf16[16,4,256]{2,1,0:T(4,128)(2,1)S(1)}, u32[]{:S(2)}, u32[]{:S(2)}) %all-to-all-start.4) | async-done | bytes 32800 | tf_op jit(solution)/shard_map/all_to_all | solution.py:94
  172.8 0.1 multiply_reduce_fusion
  173.0 39.4 %all-gather.2 = bf16[16,4,4096]{2,1,0:T(4,128)(2,1)S(1)} all-gather(bf16[1,4,4096]{2,1,0:T(4,128)(2,1)S(1)} %fusion.22), channel_id=1, replica_groups=mesh['ep'=16,'tp'=2] {'ep'}, dimensions={0}, use_global_device_ids=true | all-gather | bytes 557056 | tf_op jit(solution)/shard_map/all_gather | solution.py:99
  212.5 2.0 fusion.3
  214.6 3.8 %convolution_convert_fusion = bf16[64,4096]{1,0:T(8,128)(2,1)} fusion(bf16[1,256,4096]{2,1,0:T(8,128)(2,1)S(1)} %copy-done, bf16[64,4096]{1,0:T(8,128)(2,1)S(1)} %reshape.137, bf16[1,4096,256]{2,1,0:T(8,128)(2,1)} %param.34, f32[64,256]{1,0:T(8,128)S(1)} %fusion.3), kind=kOutput, calls=%fused_computation.1 | convolution fusion | flops 268795904 | bytes 5308416 | tf_op jit(solution)/shard_map/dot_general | solution.py:12
  218.4 1.2 convert_multiply_fusion
  219.6 1.9 reshape.118
  221.4 1.9 copy.132
  223.4 1.3 reshape.119
  224.7 46.8 %all-reduce.2 = bf16[128,2048]{1,0:T(8,128)(2,1)S(1)} all-reduce(f32[128,2048]{1,0:T(8,128)} %reshape.119), channel_id=2, replica_groups=mesh['ep'=16,'tp'=2] {'ep','tp'}, use_global_device_ids=true, to_apply=%region_5.6.clone | all-reduce | flops 262144 | bytes 1572864
  271.5 1.8 all_gather.15
  273.4 0.6 add_convert_fusion
  (58 shorter events, 2.5 us)
Async XLA Ops:
  0.6 214.0 %copy-start = (bf16[1,256,4096]{2,1,0:T(8,128)(2,1)S(1)}, bf16[1,256,4096]{2,1,0:T(8,128)(2,1)}, u32[]{:S(2)}) copy-start(bf16[1,256,4096]{2,1,0:T(8,128)(2,1)} %param.35) | copy-start | bytes 6291460
  0.6 83.0 %copy-start.5 = (f32[4,4,256]{2,1,0:T(4,128)S(1)}, f32[4,4,256]{2,1,0:T(4,128)}, u32[]{:S(2)}) copy-start(f32[4,4,256]{2,1,0:T(4,128)} %param.21) | copy-start | bytes 49156
  50.3 15.3 %all-to-all-start.1 = ((bf16[16,2,128]{2,1,0:T(2,128)(2,1)}), bf16[16,2,128]{2,1,0:T(2,128)(2,1)S(1)}, u32[]{:S(2)}, u32[]{:S(2)}) async-start(bf16[16,2,128]{2,1,0:T(2,128)(2,1)} %reshape.153), calls=%async_computation.1 | async-start | bytes 16384 | tf_op jit(solution)/shard_map/all_to_all | solution.py:69
  56.5 42.0 %copy-start.6 = (f32[4,4]{1,0:T(4,128)}, f32[4,4]{1,0:T(4,128)S(1)}, u32[]{:S(2)}) copy-start(f32[4,4]{1,0:T(4,128)S(1)} %get-tuple-element.7) | copy-start | bytes 196
  65.6 14.1 %all-to-all-start = ((bf16[16,2,128]{2,1,0:T(2,128)(2,1)}), bf16[16,2,128]{2,1,0:T(2,128)(2,1)S(1)}, u32[]{:S(2)}, u32[]{:S(2)}) async-start(bf16[16,2,128]{2,1,0:T(2,128)(2,1)} %reshape.149), calls=%async_computation | async-start | bytes 16384 | tf_op jit(solution)/shard_map/all_to_all | solution.py:68
  79.7 10.9 %all-to-all-start.2 = ((bf16[16,2,256]{2,1,0:T(2,128)(2,1)}), bf16[16,2,256]{2,1,0:T(2,128)(2,1)S(1)}, u32[]{:S(2)}, u32[]{:S(2)}) async-start(bf16[16,2,256]{2,1,0:T(2,128)(2,1)} %reshape.151), calls=%async_computation.2 | async-start | bytes 32768 | tf_op jit(solution)/shard_map/all_to_all | solution.py:70
  90.6 15.5 %all-to-all-start.3 = ((bf16[16,2,256]{2,1,0:T(2,128)(2,1)}), bf16[16,2,256]{2,1,0:T(2,128)(2,1)S(1)}, u32[]{:S(2)}, u32[]{:S(2)}) async-start(bf16[16,2,256]{2,1,0:T(2,128)(2,1)} %reshape.155), calls=%async_computation.3 | async-start | bytes 32768 | tf_op jit(solution)/shard_map/all_to_all | solution.py:71
  98.5 3.4 %copy-start.1 = (f32[4,4,256,512]{3,2,1,0:T(8,128)}, f32[4,4,256,512]{3,2,1,0:T(8,128)S(1)}, u32[]{:S(2)}) copy-start(f32[4,4,256,512]{3,2,1,0:T(8,128)S(1)} %multiply_add_fusion) | copy-start | bytes 25165828
  101.9 54.7 %copy-start.3 = (bf16[2048,256]{1,0:T(8,128)(2,1)S(1)}, bf16[2048,256]{1,0:T(8,128)(2,1)}, u32[]{:S(2)}) copy-start(bf16[2048,256]{1,0:T(8,128)(2,1)} %param.31) | copy-start | bytes 3145732
  101.9 70.8 %copy-start.2 = (bf16[4,4096]{1,0:T(4,128)(2,1)S(1)}, bf16[4,4096]{1,0:T(4,128)(2,1)}, u32[]{:S(2)}) copy-start(bf16[4,4096]{1,0:T(4,128)(2,1)} %param.19) | copy-start | bytes 98308
  101.9 71.0 %copy-start.4 = (f32[4096]{0:T(1024)S(1)}, f32[4096]{0:T(1024)}, u32[]{:S(2)}) copy-start(f32[4096]{0:T(1024)} %param.32) | copy-start | bytes 49156
  106.1 55.8 %all-to-all-start.5 = ((f32[4,16,1]{0,2,1:T(1,128)}), f32[4,16,1]{0,2,1:T(1,128)S(1)}, u32[]{:S(2)}, u32[]{:S(2)}) async-start(f32[4,16,1]{0,2,1:T(1,128)} %copy.131), calls=%async_computation.5 | async-start | bytes 16384 | tf_op jit(solution)/shard_map/all_to_all | solution.py:109
  161.9 10.9 %all-to-all-start.4 = ((bf16[16,4,256]{2,1,0:T(4,128)(2,1)}), bf16[16,4,256]{2,1,0:T(4,128)(2,1)S(1)}, u32[]{:S(2)}, u32[]{:S(2)}) async-start(bf16[16,4,256]{2,1,0:T(4,128)(2,1)} %psum.7), calls=%async_computation.4 | async-start | bytes 65536 | tf_op jit(solution)/shard_map/all_to_all | solution.py:94
where the time goes:
time: 275 us; the launch traced here: 274 us
  blocking collectives  180 us (65%)
  starting transfers between devices  27.7 us (10%)
  waiting for transfers between devices  20.3 us (7%)
  matrix products  19 us (7%)
  local copies, waits for them, and re-layouts  15.6 us (6%)
  other arithmetic  10.7 us (4%)
    unnamed x1, blocking collectives  46.8 us
    all_gather x1, blocking collectives, body(): piece = lax.all_gather(normed, 'ep', axis=0, tiled=True)  45.3 us
    all_gather x1, blocking collectives, body(): lax.all_gather(hidden, 'ep', axis=0, tiled=True)  42.4 us
    all_gather x1, blocking collectives, body(): piece = lax.all_gather(ffn_in, 'ep', axis=0, tiled=True)  39.4 us
    dot_general x9, matrix products, product(): return jnp.dot(left, right, preferred_element_type=jnp.float32)  15 us
    unnamed x26, local copies, waits for them, and re-layouts  7.67 us
    all_to_all x1, waiting for transfers between devices, body(): lax.all_to_all(summed, 'ep', split_axis=0, concat_axis=1, tiled=True)  7.25 us
    all_to_all x1, waiting for transfers between devices, body(): lax.all_to_all(query_part, 'ep', split_axis=0, concat_axis=2, tiled=True)  6.95 us
  transfers between devices with their start and end apart: 6, of which 3 were waited for; matrix products, arithmetic and copies ran while one was open for 9% of the time, Pallas kernels for 0%

commit v1 on v0

--- a/solution.py
+++ b/solution.py
@@ -2,6 +2,18 @@
 import jax.numpy as jnp
 from jax import lax
 from jax.sharding import PartitionSpec as P
+
+
+def gather_by_bits(x, axis, dim):
+    ways, here = (lax.axis_size(axis), lax.axis_index(axis))
+    grown, reach = (x, 1)
+    while reach < ways:
+        theirs = lax.ppermute(grown, axis, [(d, d ^ reach) for d in range(ways)])
+        mine_first = jnp.concatenate([grown, theirs], axis=dim)
+        theirs_first = jnp.concatenate([theirs, grown], axis=dim)
+        grown = jnp.where(here & reach == 0, mine_first, theirs_first)
+        reach = 2 * reach
+    return grown
 
 
 def rms_scale(values, gain):
@@ -89,7 +101,7 @@
         hidden.reshape(seqs, value_width)
         * jax.nn.sigmoid(outgate.reshape(seqs, value_width).astype(jnp.float32))
     ).astype(jnp.bfloat16)
-    partial_value = product(lax.all_gather(hidden, "ep", axis=0, tiled=True), w_out)
+    partial_value = product(gather_by_bits(hidden, "ep", 0), w_out)
     summed = lax.psum(rounded_term(partial_value).astype(jnp.bfloat16), "tp")
     mixed = lax.all_to_all(summed, "ep", split_axis=0, concat_axis=1, tiled=True)
     resid = tokens.astype(jnp.float32) + mixed.astype(jnp.float32)

time: 275 us -> 248 us (0.902)
  blocking collectives: 180 us -> 137 us
  waiting for transfers between devices: 20.3 us -> 28.6 us
  starting transfers between devices: 27.7 us -> 35.7 us
    all_gather x1 -> x0, blocking collectives: 42.4 us -> none  [body(): lax.all_gather(hidden, 'ep', axis=0, tiled=True)]
    ppermute x0 -> x4, starting transfers between devices: none -> 8.46 us  [gather_by_bits(): theirs = lax.ppermute(grown, axis, [(d, d ^ reach) for d in range(ways)])]
    ppermute x0 -> x4, waiting for transfers between devices: none -> 6.48 us  [gather_by_bits(): theirs = lax.ppermute(grown, axis, [(d, d ^ reach) for d in range(ways)])]
    unnamed x26 -> x27, local copies, waits for them, and re-layouts: 7.67 us -> 6.92 us
  transfers between devices with their start and end apart: 6 -> 10, of which waited for: 3 -> 7; matrix products, arithmetic and copies ran while one was open for 9% -> 9% of each run, Pallas kernels for 0% -> 0%
where the time goes in v1:
time: 248 us; the launch traced here: 247 us
  blocking collectives  137 us (55%)
  starting transfers between devices  35.7 us (14%)
  waiting for transfers between devices  28.6 us (12%)
  matrix products  19.3 us (8%)
  local copies, waits for them, and re-layouts  14.8 us (6%)
  other arithmetic  10 us (4%)
    unnamed x1, blocking collectives  47 us
    all_gather x1, blocking collectives, body(): piece = lax.all_gather(normed, 'ep', axis=0, tiled=True)  45.3 us
    all_gather x1, blocking collectives, body(): piece = lax.all_gather(ffn_in, 'ep', axis=0, tiled=True)  39.3 us
    dot_general x9, matrix products, product(): return jnp.dot(left, right, preferred_element_type=jnp.float32)  15.3 us
    ppermute x4, starting transfers between devices, gather_by_bits(): theirs = lax.ppermute(grown, axis, [(d, d ^ reach) for d in range(ways)])  8.46 us
    all_to_all x1, waiting for transfers between devices, body(): lax.all_to_all(summed, 'ep', split_axis=0, concat_axis=1, tiled=True)  7.28 us
    all_to_all x1, waiting for transfers between devices, body(): lax.all_to_all(query_part, 'ep', split_axis=0, concat_axis=2, tiled=True)  6.95 us
    unnamed x27, local copies, waits for them, and re-layouts  6.92 us
  transfers between devices with their start and end apart: 10, of which 7 were waited for; matrix products, arithmetic and copies ran while one was open for 9% of the time, Pallas kernels for 0%

profile of v1, /device:TPU:0, one launch (start us, length us, event | category | flops | bytes accessed | tf_op | source)
XLA Modules:
  0.0 246.9 jit_solution(17005531943680710488)
XLA Ops:
  0.7 1.1 fusion.20
  1.7 0.9 fusion.54
  2.6 45.3 %all-gather = bf16[16,4,4096]{2,1,0:T(4,128)(2,1)S(1)} all-gather(bf16[1,4,4096]{2,1,0:T(4,128)(2,1)S(1)} %fusion.54), channel_id=1, replica_groups=mesh['ep'=16,'tp'=2] {'ep'}, dimensions={0}, use_global_device_ids=true | all-gather | bytes 557056 | tf_op jit(solution)/shard_map/all_gather | solution.py:62
  48.0 1.3 convolution_convert_fusion.4
  49.6 0.7 reshape.151
  50.3 3.5 %all-to-all-start.1 = ((bf16[16,2,128]{2,1,0:T(2,128)(2,1)}), bf16[16,2,128]{2,1,0:T(2,128)(2,1)S(1)}, u32[]{:S(2)}, u32[]{:S(2)}) async-start(bf16[16,2,128]{2,1,0:T(2,128)(2,1)} %reshape.151), calls=%async_computation.1 | async-start | bytes 16384 | tf_op jit(solution)/shard_map/all_to_all | solution.py:81
  53.8 0.8 fusion.22
  54.6 1.3 convolution_convert_fusion.5
  56.0 1.7 convolution_convert_fusion.3
  57.7 1.7 convolution_convert_fusion.2
  59.4 0.9 fusion.35
  60.3 1.0 subtract_exponential_fusion.1
  61.5 0.7 reshape.147
  62.5 0.7 reshape.149
  63.4 0.7 reshape.153
  64.1 6.9 %all-to-all-start = ((bf16[16,2,128]{2,1,0:T(2,128)(2,1)}), bf16[16,2,128]{2,1,0:T(2,128)(2,1)S(1)}, u32[]{:S(2)}, u32[]{:S(2)}) async-start(bf16[16,2,128]{2,1,0:T(2,128)(2,1)} %reshape.147), calls=%async_computation | async-start | bytes 16384 | tf_op jit(solution)/shard_map/all_to_all | solution.py:80
  71.3 7.0 %all-to-all-done = bf16[16,2,128]{2,1,0:T(2,128)(2,1)S(1)} async-done(((bf16[16,2,128]{2,1,0:T(2,128)(2,1)}), bf16[16,2,128]{2,1,0:T(2,128)(2,1)S(1)}, u32[]{:S(2)}, u32[]{:S(2)}) %all-to-all-start) | async-done | bytes 8224 | tf_op jit(solution)/shard_map/all_to_all | solution.py:80
  78.2 3.5 %all-to-all-start.2 = ((bf16[16,2,256]{2,1,0:T(2,128)(2,1)}), bf16[16,2,256]{2,1,0:T(2,128)(2,1)S(1)}, u32[]{:S(2)}, u32[]{:S(2)}) async-start(bf16[16,2,256]{2,1,0:T(2,128)(2,1)} %reshape.149), calls=%async_computation.2 | async-start | bytes 32768 | tf_op jit(solution)/shard_map/all_to_all | solution.py:82
  82.2 0.7 multiply_reduce_fusion.1
  83.0 6.1 %all-to-all-done.2 = bf16[16,2,256]{2,1,0:T(2,128)(2,1)S(1)} async-done(((bf16[16,2,256]{2,1,0:T(2,128)(2,1)}), bf16[16,2,256]{2,1,0:T(2,128)(2,1)S(1)}, u32[]{:S(2)}, u32[]{:S(2)}) %all-to-all-start.2) | async-done | bytes 16416 | tf_op jit(solution)/shard_map/all_to_all | solution.py:82
  89.1 3.5 %all-to-all-start.3 = ((bf16[16,2,256]{2,1,0:T(2,128)(2,1)}), bf16[16,2,256]{2,1,0:T(2,128)(2,1)S(1)}, u32[]{:S(2)}, u32[]{:S(2)}) async-start(bf16[16,2,256]{2,1,0:T(2,128)(2,1)} %reshape.153), calls=%async_computation.3 | async-start | bytes 32768 | tf_op jit(solution)/shard_map/all_to_all | solution.py:83
  92.9 4.2 %multiply_add_fusion = f32[4,4,256,512]{3,2,1,0:T(8,128)S(1)} fusion(f32[4,4,256,512]{3,2,1,0:T(8,128)} %param.20, f32[4,4,512]{2,1,0:T(4,128)S(1)} %reshape.121, f32[4,4,256]{2,1,0:T(4,128)S(1)} %reshape.120, f32[4,4]{1,0:T(4,128)S(1)} %subtract_exponential_fusion, f32[4,4]{1,0:T(4,128)S(1)} %get-tuple-element.6), kind=kLoop, calls=%fused_computation | loop fusion | flops 8388608 | bytes 16826496 | tf_op jit(solution)/shard_map/add | solution.py:93
  97.1 3.4 %copy-done.1 = f32[4,4,256,512]{3,2,1,0:T(8,128)} copy-done((f32[4,4,256,512]{3,2,1,0:T(8,128)}, f32[4,4,256,512]{3,2,1,0:T(8,128)S(1)}, u32[]{:S(2)}) %copy-start.1) | copy-done | bytes 8388632
  100.5 4.0 %fusion.36 = f32[4,4,1,512]{3,2,1,0:T(1,128)S(1)} fusion(f32[4,4,256,1]{2,3,1,0:T(1,128)S(1)} %reshape.139, f32[4,4,256,512]{3,2,1,0:T(8,128)S(1)} %multiply_add_fusion), kind=kOutput, calls=%fused_computation.67 | convolution fusion | flops 25165824 | bytes 8437760 | tf_op jit(solution)/shard_map/shd,shde->she/dot_general | solution.py:97
  105.1 1.9 collective-permute-start
  107.0 1.9 collective-permute-done
  109.0 1.9 collective-permute-start.1
  110.9 2.1 collective-permute-done.1
  113.0 1.9 collective-permute-start.2
  114.9 2.4 collective-permute-done.2
  117.3 2.8 %collective-permute-start.3 = (bf16[32,2048]{1,0:T(8,128)(2,1)S(1)}, bf16[32,2048]{1,0:T(8,128)(2,1)S(1)}, u32[]{:S(2)}, u32[]{:S(2)}) collective-permute-start(bf16[32,2048]{1,0:T(8,128)(2,1)S(1)} %maximum_select_fusion.2), channel_id=1, source_target_pairs={{0,16},{2,18},{4,20},{6,22},{8,24},{10,26},{12,28},{14,30},{16,0},... | collective-permute-start | bytes 393224 | tf_op jit(solution)/shard_map/ppermute | solution.py:11
  120.2 0.7 copy.131
  120.9 4.7 %all-to-all-start.5 = ((f32[4,16,1]{0,2,1:T(1,128)}), f32[4,16,1]{0,2,1:T(1,128)S(1)}, u32[]{:S(2)}, u32[]{:S(2)}) async-start(f32[4,16,1]{0,2,1:T(1,128)} %copy.131), calls=%async_computation.5 | async-start | bytes 16384 | tf_op jit(solution)/shard_map/all_to_all | solution.py:121
  125.7 1.5 convolution_convert_fusion.1
  127.2 4.0 %psum.7 = bf16[16,4,256]{2,1,0:T(4,128)(2,1)} all-reduce(bf16[16,4,256]{2,1,0:T(4,128)(2,1)S(1)} %all_to_all.24), channel_id=1, replica_groups=mesh['ep'=16,'tp'=2] {'tp'}, use_global_device_ids=true, to_apply=%region_2.3 | all-reduce | flops 16384 | bytes 65536 | tf_op jit(solution)/shard_map/psum | solution.py:105
  131.2 1.7 all-to-all-done.5
  133.0 5.2 %all-to-all-start.4 = ((bf16[16,4,256]{2,1,0:T(4,128)(2,1)}), bf16[16,4,256]{2,1,0:T(4,128)(2,1)S(1)}, u32[]{:S(2)}, u32[]{:S(2)}) async-start(bf16[16,4,256]{2,1,0:T(4,128)(2,1)} %psum.7), calls=%async_computation.4 | async-start | bytes 65536 | tf_op jit(solution)/shard_map/all_to_all | solution.py:106
  138.2 7.3 %all-to-all-done.4 = bf16[16,4,256]{2,1,0:T(4,128)(2,1)S(1)} async-done(((bf16[16,4,256]{2,1,0:T(4,128)(2,1)}), bf16[16,4,256]{2,1,0:T(4,128)(2,1)S(1)}, u32[]{:S(2)}, u32[]{:S(2)}) %all-to-all-start.4) | async-done | bytes 32800 | tf_op jit(solution)/shard_map/all_to_all | solution.py:106
  145.8 39.3 %all-gather.1 = bf16[16,4,4096]{2,1,0:T(4,128)(2,1)S(1)} all-gather(bf16[1,4,4096]{2,1,0:T(4,128)(2,1)S(1)} %fusion.28), channel_id=1, replica_groups=mesh['ep'=16,'tp'=2] {'ep'}, dimensions={0}, use_global_device_ids=true | all-gather | bytes 557056 | tf_op jit(solution)/shard_map/all_gather | solution.py:111
  185.2 2.0 fusion.3
  187.3 3.8 %convolution_convert_fusion = bf16[64,4096]{1,0:T(8,128)(2,1)} fusion(bf16[1,256,4096]{2,1,0:T(8,128)(2,1)S(1)} %copy-done, bf16[64,4096]{1,0:T(8,128)(2,1)S(1)} %reshape.135, bf16[1,4096,256]{2,1,0:T(8,128)(2,1)} %param.34, f32[64,256]{1,0:T(8,128)S(1)} %fusion.3), kind=kOutput, calls=%fused_computation.1 | convolution fusion | flops 268795904 | bytes 5308416 | tf_op jit(solution)/shard_map/dot_general | solution.py:24
  191.0 1.2 convert_multiply_fusion
  192.2 1.9 reshape.118
  194.1 1.9 copy.132
  196.0 1.3 reshape.119
  197.4 47.0 %all-reduce.2 = bf16[128,2048]{1,0:T(8,128)(2,1)S(1)} all-reduce(f32[128,2048]{1,0:T(8,128)} %reshape.119), channel_id=2, replica_groups=mesh['ep'=16,'tp'=2] {'ep','tp'}, use_global_device_ids=true, to_apply=%region_5.6.clone | all-reduce | flops 262144 | bytes 1572864
  244.4 1.8 all_gather.11
  246.2 0.6 add_convert_fusion
  (69 shorter events, 3.3 us)
Async XLA Ops:
  0.6 186.6 %copy-start = (bf16[1,256,4096]{2,1,0:T(8,128)(2,1)S(1)}, bf16[1,256,4096]{2,1,0:T(8,128)(2,1)}, u32[]{:S(2)}) copy-start(bf16[1,256,4096]{2,1,0:T(8,128)(2,1)} %param.35) | copy-start | bytes 6291460
  0.6 81.5 %copy-start.4 = (f32[4,4,256]{2,1,0:T(4,128)S(1)}, f32[4,4,256]{2,1,0:T(4,128)}, u32[]{:S(2)}) copy-start(f32[4,4,256]{2,1,0:T(4,128)} %param.21) | copy-start | bytes 49156
  50.3 13.8 %all-to-all-start.1 = ((bf16[16,2,128]{2,1,0:T(2,128)(2,1)}), bf16[16,2,128]{2,1,0:T(2,128)(2,1)S(1)}, u32[]{:S(2)}, u32[]{:S(2)}) async-start(bf16[16,2,128]{2,1,0:T(2,128)(2,1)} %reshape.151), calls=%async_computation.1 | async-start | bytes 16384 | tf_op jit(solution)/shard_map/all_to_all | solution.py:81
  61.3 35.8 %copy-start.5 = (f32[4,4]{1,0:T(4,128)}, f32[4,4]{1,0:T(4,128)S(1)}, u32[]{:S(2)}) copy-start(f32[4,4]{1,0:T(4,128)S(1)} %get-tuple-element.7) | copy-start | bytes 196
  64.1 14.1 %all-to-all-start = ((bf16[16,2,128]{2,1,0:T(2,128)(2,1)}), bf16[16,2,128]{2,1,0:T(2,128)(2,1)S(1)}, u32[]{:S(2)}, u32[]{:S(2)}) async-start(bf16[16,2,128]{2,1,0:T(2,128)(2,1)} %reshape.147), calls=%async_computation | async-start | bytes 16384 | tf_op jit(solution)/shard_map/all_to_all | solution.py:80
  78.2 10.9 %all-to-all-start.2 = ((bf16[16,2,256]{2,1,0:T(2,128)(2,1)}), bf16[16,2,256]{2,1,0:T(2,128)(2,1)S(1)}, u32[]{:S(2)}, u32[]{:S(2)}) async-start(bf16[16,2,256]{2,1,0:T(2,128)(2,1)} %reshape.149), calls=%async_computation.2 | async-start | bytes 32768 | tf_op jit(solution)/shard_map/all_to_all | solution.py:82
  89.1 15.5 %all-to-all-start.3 = ((bf16[16,2,256]{2,1,0:T(2,128)(2,1)}), bf16[16,2,256]{2,1,0:T(2,128)(2,1)S(1)}, u32[]{:S(2)}, u32[]{:S(2)}) async-start(bf16[16,2,256]{2,1,0:T(2,128)(2,1)} %reshape.153), calls=%async_computation.3 | async-start | bytes 32768 | tf_op jit(solution)/shard_map/all_to_all | solution.py:83
  97.1 3.4 %copy-start.1 = (f32[4,4,256,512]{3,2,1,0:T(8,128)}, f32[4,4,256,512]{3,2,1,0:T(8,128)S(1)}, u32[]{:S(2)}) copy-start(f32[4,4,256,512]{3,2,1,0:T(8,128)S(1)} %multiply_add_fusion) | copy-start | bytes 25165828
  100.5 19.7 %copy-start.6 = (f32[4,2]{0,1:T(2,128)S(1)}, f32[4,2]{0,1:T(2,128)}, u32[]{:S(2)}) copy-start(f32[4,2]{0,1:T(2,128)} %param.37) | copy-start | bytes 100
  100.5 19.7 %copy-start.7 = (s32[4,2]{0,1:T(2,128)S(1)}, s32[4,2]{0,1:T(2,128)}, u32[]{:S(2)}) copy-start(s32[4,2]{0,1:T(2,128)} %param.36) | copy-start | bytes 100
  100.5 45.1 %copy-start.2 = (bf16[4,4096]{1,0:T(4,128)(2,1)S(1)}, bf16[4,4096]{1,0:T(4,128)(2,1)}, u32[]{:S(2)}) copy-start(bf16[4,4096]{1,0:T(4,128)(2,1)} %param.19) | copy-start | bytes 98308
  100.5 45.2 %copy-start.3 = (f32[4096]{0:T(1024)S(1)}, f32[4096]{0:T(1024)}, u32[]{:S(2)}) copy-start(f32[4096]{0:T(1024)} %param.32) | copy-start | bytes 49156
  105.1 3.8 %collective-permute-start = (bf16[4,2048]{1,0:T(4,128)(2,1)S(1)}, bf16[4,2048]{1,0:T(4,128)(2,1)S(1)}, u32[]{:S(2)}, u32[]{:S(2)}) collective-permute-start(bf16[4,2048]{1,0:T(4,128)(2,1)S(1)} %multiply_convert_fusion.1), channel_id=1, source_target_pairs={{0,2},{2,0},{4,6},{6,4},{8,10},{10,8},{12,14},{14,12},{16,18},{18,... | collective-permute-start | bytes 49160 | tf_op jit(solution)/shard_map/ppermute | solution.py:11
  109.0 4.0 %collective-permute-start.1 = (bf16[8,2048]{1,0:T(8,128)(2,1)S(1)}, bf16[8,2048]{1,0:T(8,128)(2,1)S(1)}, u32[]{:S(2)}, u32[]{:S(2)}) collective-permute-start(bf16[8,2048]{1,0:T(8,128)(2,1)S(1)} %maximum_select_fusion.4), channel_id=1, source_target_pairs={{0,4},{2,6},{4,0},{6,2},{8,12},{10,14},{12,8},{14,10},{16,20},{18,... | collective-permute-start | bytes 98312 | tf_op jit(solution)/shard_map/ppermute | solution.py:11
  113.0 4.3 %collective-permute-start.2 = (bf16[16,2048]{1,0:T(8,128)(2,1)S(1)}, bf16[16,2048]{1,0:T(8,128)(2,1)S(1)}, u32[]{:S(2)}, u32[]{:S(2)}) collective-permute-start(bf16[16,2048]{1,0:T(8,128)(2,1)S(1)} %maximum_select_fusion.3), channel_id=1, source_target_pairs={{0,8},{2,10},{4,12},{6,14},{8,0},{10,2},{12,4},{14,6},{16,24},{18,... | collective-permute-start | bytes 196616 | tf_op jit(solution)/shard_map/ppermute | solution.py:11
  117.3 8.3 %collective-permute-start.3 = (bf16[32,2048]{1,0:T(8,128)(2,1)S(1)}, bf16[32,2048]{1,0:T(8,128)(2,1)S(1)}, u32[]{:S(2)}, u32[]{:S(2)}) collective-permute-start(bf16[32,2048]{1,0:T(8,128)(2,1)S(1)} %maximum_select_fusion.2), channel_id=1, source_target_pairs={{0,16},{2,18},{4,20},{6,22},{8,24},{10,26},{12,28},{14,30},{16,0},... | collective-permute-start | bytes 393224 | tf_op jit(solution)/shard_map/ppermute | solution.py:11
  120.9 12.0 %all-to-all-start.5 = ((f32[4,16,1]{0,2,1:T(1,128)}), f32[4,16,1]{0,2,1:T(1,128)S(1)}, u32[]{:S(2)}, u32[]{:S(2)}) async-start(f32[4,16,1]{0,2,1:T(1,128)} %copy.131), calls=%async_computation.5 | async-start | bytes 16384 | tf_op jit(solution)/shard_map/all_to_all | solution.py:121
  133.0 12.6 %all-to-all-start.4 = ((bf16[16,4,256]{2,1,0:T(4,128)(2,1)}), bf16[16,4,256]{2,1,0:T(4,128)(2,1)S(1)}, u32[]{:S(2)}, u32[]{:S(2)}) async-start(bf16[16,4,256]{2,1,0:T(4,128)(2,1)} %psum.7), calls=%async_computation.4 | async-start | bytes 65536 | tf_op jit(solution)/shard_map/all_to_all | solution.py:106
